TPU v7x, 32 devices: a whole 2x2x4 slice. The times are simulated.
32 devices in a mesh: ep: 8 (over z, x), tp: 4 (over y, core).
Axes of the slice: x: 2, y: 2, z: 4, core: 2. Of those that a mesh axis runs over, the one named last changes fastest.
Arguments:
- tokens: bfloat16 [256, 2048], P('ep'), may hold values from -24 to 24
- norm_gain: float32 [2048], replicated, may hold values from 0.1 to 1.9
- post_gain: float32 [2048], replicated, may hold values from 0.1 to 1.9
- w_query: bfloat16 [2048, 2048], P(None, 'tp'), may hold values from -0.125 to 0.125
- w_key: bfloat16 [2048, 512], P(None, 'tp'), may hold values from -0.125 to 0.125
- w_value: bfloat16 [2048, 512], P(None, 'tp'), may hold values from -0.125 to 0.125
- w_forget: bfloat16 [2048, 32], replicated, may hold values from -0.25 to 0.25
- w_output: bfloat16 [2048, 2048], P('tp'), may hold values from -0.125 to 0.125
- key_cache: bfloat16 [256, 8, 64, 1024], P('ep', 'tp'), may hold values from -660 to 660
- value_cache: bfloat16 [256, 8, 64, 1024], P('ep', 'tp'), may hold values from -6 to 6
- gate_cache: float32 [256, 32, 1024], P('ep', 'tp'), may hold values from -176.08 to 0, as said below
- lengths: int32 [256], P('ep'), may hold values from 256 to 1024
- routes: int32 [256, 2], P('ep'), may hold values from 0 to 7, all different within a row; in each aligned block of 32 rows (0 to 31, 32 to 63, ...) at most 16 rows name the same one
- route_logits: float32 [256, 2], P('ep'), may hold values from -6 to 6
- w_gate: bfloat16 [8, 2048, 3584], P('ep', None, 'tp'), may hold values from -0.125 to 0.125
- w_up: bfloat16 [8, 2048, 3584], P('ep', None, 'tp'), may hold values from -0.125 to 0.125
- w_down: bfloat16 [8, 3584, 2048], P('ep', 'tp'), may hold values from -0.09375 to 0.09375
Outputs:
- layer_out: bfloat16 [256, 2048], P('ep', 'tp')
Inputs may be any that keep to these rules, and one draw needn't show every extreme that they name: `routes`: each row names 2 different experts. The rows of one index of ep name any one expert at most 16 times, and in every draw some index of ep names some expert exactly 16 times. `gate_cache`: cumulative sums of negative log forget gates along positions: nonincreasing along the last dimension. `lengths`: the new token follows the valid positions of its sequence.
All inputs are finite; a program needn't handle non-finite values.
Results may differ from a plain program's by a relative error of at most 0.011.
Values may be sent and summed in bfloat16 or wider, within the bound.
No kernel may reach another device: no remote copies, remote signals or barrier semaphores. Data moves between devices by JAX's collectives and lax.ppermute only.
A program may use at most 64 MiB of HBM per device.

v0:
```python
import jax
import jax.numpy as jnp
from jax import lax
from jax.sharding import PartitionSpec as P

epsilon = 1e-06


def body(
    tokens,
    norm_gain,
    post_gain,
    w_query,
    w_key,
    w_value,
    w_forget,
    w_output,
    key_cache,
    value_cache,
    gate_cache,
    lengths,
    routes,
    route_logits,
    w_gate,
    w_up,
    w_down,
):
    ep_count = lax.axis_size("ep")
    tp_count = lax.axis_size("tp")
    tp_index = lax.axis_index("tp")
    seq_count, width = tokens.shape
    kv_local, head_dim, cache_span = (key_cache.shape[1], key_cache.shape[2], key_cache.shape[3])
    heads_local = gate_cache.shape[1]
    group_size = heads_local // kv_local
    own_width = width // tp_count
    column_start = tp_index * own_width
    tokens_wide = tokens.astype(jnp.float32)
    normed = (
        tokens_wide
        * lax.rsqrt(jnp.mean(tokens_wide * tokens_wide, axis=-1, keepdims=True) + epsilon)
        * norm_gain
    ).astype(jnp.bfloat16)
    forget_columns = lax.dynamic_slice_in_dim(w_forget, tp_index * heads_local, heads_local, 1)
    log_forget = jax.nn.log_sigmoid(
        jnp.dot(normed, forget_columns, preferred_element_type=jnp.float32)
    )
    query_vector = jnp.dot(normed, w_query, preferred_element_type=jnp.float32).astype(jnp.bfloat16)
    fresh_key = jnp.dot(normed, w_key, preferred_element_type=jnp.float32).astype(jnp.bfloat16)
    value_new = jnp.dot(normed, w_value, preferred_element_type=jnp.float32).astype(jnp.bfloat16)
    query_vector = query_vector.reshape(seq_count, kv_local, group_size, head_dim)
    fresh_key = fresh_key.reshape(seq_count, kv_local, head_dim)
    value_new = value_new.reshape(seq_count, kv_local, head_dim)
    score_scale = head_dim ** (-0.5)
    past_scores = jnp.einsum(
        "bkgd,bkdl->bkgl", query_vector, key_cache, preferred_element_type=jnp.float32
    ).reshape(seq_count, heads_local, cache_span)
    cache_position = lax.broadcasted_iota(jnp.int32, (1, 1, cache_span), 2)
    last_index = (lengths - 1)[:, None, None]
    latest = jnp.sum(jnp.where(cache_position == last_index, gate_cache, 0.0), axis=-1)
    past_scores = past_scores * score_scale + (latest + log_forget)[:, :, None] - gate_cache
    past_scores = jnp.where(cache_position < lengths[:, None, None], past_scores, -jnp.inf)
    new_score = (
        jnp.einsum(
            "rlse,rle->rls", query_vector, fresh_key, preferred_element_type=jnp.float32
        ).reshape(seq_count, heads_local)
        * score_scale
    )
    peak_score = jnp.maximum(jnp.max(past_scores, axis=-1), new_score)
    past_exp = jnp.exp(past_scores - peak_score[:, :, None])
    new_exp = jnp.exp(new_score - peak_score)
    denominator = jnp.sum(past_exp, axis=-1) + new_exp
    past_prob = (past_exp / denominator[:, :, None]).astype(jnp.bfloat16)
    new_prob = (new_exp / denominator).astype(jnp.bfloat16)
    mixed_heads = jnp.einsum(
        "bkgl,bkdl->bkgd",
        past_prob.reshape(seq_count, kv_local, group_size, cache_span),
        value_cache,
        preferred_element_type=jnp.float32,
    )
    mixed_heads = mixed_heads + new_prob.reshape(seq_count, kv_local, group_size)[
        :, :, :, None
    ].astype(jnp.float32) * value_new[:, :, None, :].astype(jnp.float32)
    attended = mixed_heads.astype(jnp.bfloat16).reshape(seq_count, heads_local * head_dim)
    partial_value = jnp.dot(attended, w_output, preferred_element_type=jnp.float32).astype(
        jnp.bfloat16
    )
    attention = lax.psum_scatter(partial_value, "tp", scatter_dimension=1, tiled=True).astype(
        jnp.float32
    )
    residual = lax.dynamic_slice_in_dim(tokens_wide, column_start, own_width, 1) + attention
    squares = lax.psum(jnp.sum(residual * residual, axis=-1), "tp")
    gain_part = lax.dynamic_slice_in_dim(post_gain, column_start, own_width, 0)
    expert_input = (residual * lax.rsqrt(squares / width + epsilon)[:, None] * gain_part).astype(
        jnp.bfloat16
    )
    route_width = routes.shape[1]
    route_count = seq_count * route_width
    capacity = 2 * seq_count * route_width // ep_count
    slot_count = ep_count * capacity
    flat_routes = routes.reshape(route_count)
    expert_onehot = (
        flat_routes[:, None] == lax.broadcasted_iota(jnp.int32, (1, ep_count), 1)
    ).astype(jnp.int32)
    route_rank = jnp.sum(jnp.cumsum(expert_onehot, axis=0) * expert_onehot, axis=1) - 1
    slot_index = flat_routes * capacity + route_rank
    slot_onehot = (
        slot_index[:, None] == lax.broadcasted_iota(jnp.int32, (1, slot_count), 1)
    ).astype(jnp.float32)
    token_onehot = (
        lax.broadcasted_iota(jnp.int32, (route_count, 1), 0) // route_width
        == lax.broadcasted_iota(jnp.int32, (1, seq_count), 1)
    ).astype(jnp.float32)
    dispatch = jnp.dot(slot_onehot.T, token_onehot).astype(jnp.bfloat16)
    packed = jnp.dot(dispatch, expert_input, preferred_element_type=jnp.float32).astype(
        jnp.bfloat16
    )
    sent_width = packed.shape[1]
    arrived = lax.all_to_all(
        packed.reshape(ep_count, capacity, sent_width),
        "ep",
        split_axis=0,
        concat_axis=0,
        tiled=True,
    )
    expert_rows = arrived.reshape(slot_count, sent_width)
    expert_rows = lax.all_gather(expert_rows, "tp", axis=1, tiled=True)
    gate_act = jnp.dot(expert_rows, w_gate[0], preferred_element_type=jnp.float32)
    upper = jnp.dot(expert_rows, w_up[0], preferred_element_type=jnp.float32)
    hidden_act = (jax.nn.silu(gate_act) * upper).astype(jnp.bfloat16)
    down_part = jnp.dot(hidden_act, w_down[0], preferred_element_type=jnp.float32).astype(
        jnp.bfloat16
    )
    expert_out = (
        lax.psum_scatter(down_part, "tp", scatter_dimension=1, tiled=True)
        .astype(jnp.float32)
        .astype(jnp.bfloat16)
    )
    returned = lax.all_to_all(
        expert_out.reshape(ep_count, capacity, own_width),
        "ep",
        split_axis=0,
        concat_axis=0,
        tiled=True,
    )
    route_weight = jax.nn.softmax(route_logits, axis=-1).reshape(route_count)
    combine = jnp.dot(
        token_onehot.T, slot_onehot * route_weight[:, None], precision=lax.Precision.HIGHEST
    )
    expert_mix = jnp.dot(
        combine,
        returned.reshape(slot_count, own_width).astype(jnp.float32),
        precision=lax.Precision.HIGHEST,
    )
    return (residual + expert_mix).astype(jnp.bfloat16)


def solution(mesh):
    in_specs = (
        P("ep", None),
        P(),
        P(),
        P(None, "tp"),
        P(None, "tp"),
        P(None, "tp"),
        P(),
        P("tp", None),
        P("ep", "tp", None, None),
        P("ep", "tp", None, None),
        P("ep", "tp", None),
        P("ep"),
        P("ep", None),
        P("ep", None),
        P("ep", None, "tp"),
        P("ep", None, "tp"),
        P("ep", "tp", None),
    )
    out_specs = P("ep", "tp")
    return jax.shard_map(body, mesh=mesh, in_specs=in_specs, out_specs=out_specs, check_vma=False)
```

profile of v0, /device:TPU:0, one launch (start us, length us, event | category | flops | bytes accessed | tf_op | source)
XLA Modules:
  0.0 132.9 jit_solution(5360184563448234798)
XLA Ops:
  6.5 0.8 broadcast_add_fusion
  7.3 0.7 iota_compare_fusion.1
  8.1 1.0 multiply_reduce_fusion
  9.1 0.1 iota_compare_fusion
  9.2 1.5 %select_reduce_fusion = f32[32,8]{1,0:T(8,128)S(1)} fusion(f32[32,8,1024]{2,1,0:T(8,128)} %param.27, pred[32,1024]{1,0:T(8,128)(4,1)S(1)} %iota_compare_fusion), kind=kLoop, calls=%fused_computation.25 | loop fusion | flops 524032 | bytes 1082368 | tf_op jit(solution)/shard_map/reduce_sum | solution.py:59
  10.8 1.1 fusion.43
  11.9 0.1 copy.37
  12.0 2.2 %convolution_convert_fusion.2 = bf16[32,512]{1,0:T(8,128)(2,1)S(1)} fusion(bf16[2048,512]{1,0:T(8,128)(2,1)} %param.20, f32[2048]{0:T(1024)} %param.18, f32[32]{0:T(128)S(1)} %add_rsqrt_fusion.1, bf16[32,2048]{1,0:T(8,128)(2,1)} %param.17), kind=kOutput, calls=%fused_computation.16 | convolution fusion | flops 67387392 | bytes 2269312 | tf_op jit(solution)/shard_map/dot_general | solution.py:47
  14.2 0.1 reshape.169
  14.3 4.6 %convolution_multiply_fusion = f32[32,2,4,1024]{3,2,1,0:T(4,128)S(1)} fusion(bf16[32,2,4,64]{3,2,1,0:T(4,128)(2,1)S(1)} %reshape.169, bf16[32,2,64,1024]{3,2,1,0:T(8,128)(2,1)} %param.25), kind=kOutput, calls=%fused_computation.8 | convolution fusion | flops 33816576 | bytes 9469952 | tf_op jit(solution)/shard_map/bkgd,bkdl->bkgl/dot_general | solution.py:54
  18.9 1.4 %mul.121 = f32[32,8,1024]{2,1,0:T(8,128)} reshape(f32[32,2,4,1024]{3,2,1,0:T(4,128)S(1)} %convolution_multiply_fusion) | data formatting | bytes 2097152 | tf_op jit(solution)/shard_map/mul | solution.py:60
  20.3 1.9 %fusion.54 = (f32[32,8]{1,0:T(8,128)S(1)}, f32[32,8,1024]{2,1,0:T(8,128)S(1)}) fusion(f32[32,8,1024]{2,1,0:T(8,128)} %param.27, f32[32,8,1024]{2,1,0:T(8,128)} %mul.121, f32[32,8]{1,0:T(8,128)S(1)} %copy.37, pred[32,1024]{1,0:T(8,128)(4,1)S(1)} %iota_compare_fusion.1), kind=kLoop, calls=%fused_computation.81 | loop fusion | flops 1048320 | bytes 3180544 | tf_op jit(solution)/shard_map/reduce_max | solution.py:68
  22.2 1.3 convolution_convert_fusion.5
  23.5 0.1 reshape.182
  23.6 0.2 fusion.55
  23.8 0.1 copy.48
  23.9 0.1 copy.39
  24.0 0.3 fusion.18
  24.4 0.1 copy.41
  24.5 1.1 divide_convert_fusion
  25.6 1.2 reshape.171
  26.8 0.1 copy.44
  26.9 1.3 fusion.17
  28.2 0.1 reshape.178
  28.3 5.7 %fusion.15 = bf16[32,2,4,64]{3,2,1,0:T(4,128)(2,1)S(1)} fusion(bf16[32,2,4,1024]{3,2,1,0:T(4,128)(2,1)S(1)} %reshape.171, bf16[32,2,64,1024]{3,2,1,0:T(8,128)(2,1)} %param.26, f32[32,2,64]{2,1,0:T(2,128)S(1)} %reshape.178, f32[32,2,4]{2,1,0:T(2,128)S(1)} %copy.44), kind=kOutput, calls=%fused_computation.13 | convolution fusion | flops 33603584 | bytes 8963072 | tf_op jit(solution)/shard_map/bkgl,bkdl->bkgd/dot_general | solution.py:74
  34.0 0.1 reshape.172
  34.1 1.1 convolution_convert_fusion
  35.3 0.1 copy.45
  35.4 0.1 reshape.173
  35.5 0.1 fusion.31
  35.6 0.1 reduce_window_sum.11
  35.7 0.2 select_reduce_fusion.1
  35.9 0.8 dynamic_slice.11
  36.7 21.2 %reduce-scatter.3.cloned.1.call-done = bf16[32,512]{1,0:T(8,128)(2,1)} async-done(((bf16[32,2048]{1,0:T(8,128)(2,1)}), bf16[32,512]{1,0:T(8,128)(2,1)}) %reduce-scatter.3.cloned.1.call-update) | async-done | bytes 32784 | tf_op jit(solution)/shard_map/reduce_scatter | solution.py:87
  57.8 0.9 multiply_reduce_fusion.1
  58.7 5.8 %psum.7 = f32[32]{0:T(128)S(1)} all-reduce(f32[32]{0:T(128)S(1)} %multiply_reduce_fusion.1), channel_id=1, replica_groups=mesh['ep'=8,'tp'=4] {'tp'}, use_global_device_ids=true, to_apply=%region_10.11 | all-reduce | flops 32 | bytes 256 | tf_op jit(solution)/shard_map/psum | solution.py:91
  64.5 1.2 convolution_convert_fusion.1
  65.7 12.8 %all_to_all.10 = bf16[8,16,512]{2,1,0:T(8,128)(2,1)S(1)} all-to-all(bf16[8,16,512]{2,1,0:T(8,128)(2,1)S(1)} %bitcast.46), channel_id=1, replica_groups=mesh['ep'=8,'tp'=4] {'ep'}, dimensions={0} | all-to-all | bytes 262144 | tf_op jit(solution)/shard_map/all_to_all | solution.py:118
  78.5 6.5 %all_gather.3 = bf16[128,2048]{1,0:T(8,128)(2,1)S(1)} all-gather(bf16[128,512]{1,0:T(8,128)(2,1)S(1)} %bitcast.43), channel_id=1, replica_groups=mesh['ep'=8,'tp'=4] {'tp'}, dimensions={1}, use_global_device_ids=true | all-gather | bytes 655360 | tf_op jit(solution)/shard_map/all_gather | solution.py:126
  85.0 2.8 %fusion.4 = f32[128,896]{1,0:T(8,128)S(1)} fusion(bf16[128,2048]{1,0:T(8,128)(2,1)S(1)} %all_gather.3, bf16[1,2048,896]{2,1,0:T(8,128)(2,1)} %param.31), kind=kOutput, calls=%fused_computation.4 | convolution fusion | flops 469762048 | bytes 4653056 | tf_op jit(solution)/shard_map/dot_general | solution.py:127
  87.8 5.3 %fusion.6 = bf16[128,2048]{1,0:T(8,128)(2,1)} fusion(bf16[1,896,2048]{2,1,0:T(8,128)(2,1)} %param.33, bf16[128,2048]{1,0:T(8,128)(2,1)S(1)} %all_gather.3, bf16[1,2048,896]{2,1,0:T(8,128)(2,1)} %param.32, f32[128,896]{1,0:T(8,128)S(1)} %fusion.4), kind=kOutput, calls=%fused_computation.6 | convolution fusion | flops 940474368 | bytes 8847360 | tf_op jit(solution)/shard_map/dot_general | solution.py:130
  93.2 19.3 %reduce-scatter.5.cloned.1.call-done = bf16[128,512]{1,0:T(8,128)(2,1)} async-done(((bf16[128,2048]{1,0:T(8,128)(2,1)}), bf16[128,512]{1,0:T(8,128)(2,1)}) %reduce-scatter.5.cloned.1.call-update) | async-done | bytes 131088 | tf_op jit(solution)/shard_map/reduce_scatter | solution.py:134
  112.4 5.5 %all-to-all-start.1 = ((bf16[8,16,512]{2,1,0:T(8,128)(2,1)}), bf16[8,16,512]{2,1,0:T(8,128)(2,1)S(1)}, u32[]{:S(2)}, u32[]{:S(2)}) async-start(bf16[8,16,512]{2,1,0:T(8,128)(2,1)} %bitcast.45), calls=%async_computation.3 | async-start | bytes 262144 | tf_op jit(solution)/shard_map/all_to_all | solution.py:138
  117.9 0.1 copy.46
  118.0 0.1 mul.132
  118.1 0.3 fusion.29
  118.4 6.9 %all-to-all-done.1 = bf16[8,16,512]{2,1,0:T(8,128)(2,1)S(1)} async-done(((bf16[8,16,512]{2,1,0:T(8,128)(2,1)}), bf16[8,16,512]{2,1,0:T(8,128)(2,1)S(1)}, u32[]{:S(2)}, u32[]{:S(2)}) %all-to-all-start.1) | async-done | bytes 131104 | tf_op jit(solution)/shard_map/all_to_all | solution.py:138
  125.3 0.8 fusion.16
  (30 shorter events, 0.4 us)
Async XLA Ops:
  6.5 27.6 %copy-start = (bf16[512,2048]{1,0:T(8,128)(2,1)S(1)}, bf16[512,2048]{1,0:T(8,128)(2,1)}, u32[]{:S(2)}) copy-start(bf16[512,2048]{1,0:T(8,128)(2,1)} %param.24) | copy-start | bytes 6291460
  6.5 51.3 %reduce-scatter.3.cloned.1.call-start = ((), (), s32[]{:S(2)}) async-start(), calls=%async_computation.4 | async-start | bytes 163840 | tf_op jit(solution)/shard_map/reduce_scatter | solution.py:87
  18.9 3.3 %copy-start.1 = (bf16[32,2048]{1,0:T(8,128)(2,1)S(1)}, bf16[32,2048]{1,0:T(8,128)(2,1)}, u32[]{:S(2)}) copy-start(bf16[32,2048]{1,0:T(8,128)(2,1)} %param.17) | copy-start | bytes 393220
  18.9 3.3 %copy-start.3 = (f32[2048]{0:T(1024)S(1)}, f32[2048]{0:T(1024)}, u32[]{:S(2)}) copy-start(f32[2048]{0:T(1024)} %param.18) | copy-start | bytes 24580
  28.3 7.0 %copy-start.5 = (s32[32,2]{0,1:T(2,128)S(1)}, s32[32,2]{0,1:T(2,128)}, u32[]{:S(2)}) copy-start(s32[32,2]{0,1:T(2,128)} %param.29) | copy-start | bytes 772
  35.3 77.2 %reduce-scatter.5.cloned.1.call-start = ((), (), s32[]{:S(2)}) async-start(), calls=%async_computation.5 | async-start | bytes 655360 | tf_op jit(solution)/shard_map/reduce_scatter | solution.py:134
  87.8 5.3 %copy-start.4 = (f32[32,2]{0,1:T(2,128)S(1)}, f32[32,2]{0,1:T(2,128)}, u32[]{:S(2)}) copy-start(f32[32,2]{0,1:T(2,128)} %param.30) | copy-start | bytes 772
  87.8 37.5 %copy-start.2 = (bf16[32,512]{1,0:T(8,128)(2,1)S(1)}, bf16[32,512]{1,0:T(8,128)(2,1)}, u32[]{:S(2)}) copy-start(bf16[32,512]{1,0:T(8,128)(2,1)} %reduce-scatter.3.cloned.1.call-done) | copy-start | bytes 98308
  112.4 12.8 %all-to-all-start.1 = ((bf16[8,16,512]{2,1,0:T(8,128)(2,1)}), bf16[8,16,512]{2,1,0:T(8,128)(2,1)S(1)}, u32[]{:S(2)}, u32[]{:S(2)}) async-start(bf16[8,16,512]{2,1,0:T(8,128)(2,1)} %bitcast.45), calls=%async_computation.3 | async-start | bytes 262144 | tf_op jit(solution)/shard_map/all_to_all | solution.py:138
Sparse Core Ops, SparseCore 0:
  35.4 22.4 reduce-scatter.2
  93.2 19.1 reduce-scatter.4
where the time goes:
time: 134 us; the launch traced here: 133 us
  waiting for transfers between devices  47.3 us (35%)
  matrix products  27.8 us (21%)
  blocking collectives  25.1 us (19%)
  between operations  13.6 us (10%)
  other arithmetic  8.77 us (7%)
  starting transfers between devices  5.54 us (4%)
  local copies, waits for them, and re-layouts  4.81 us (4%)
    reduce_scatter x1, waiting for transfers between devices, body(): lax.psum_scatter(partial_value, 'tp', scatter_dimension=1, tiled=True)  21.2 us
    reduce_scatter x1, waiting for transfers between devices, body(): lax.psum_scatter(down_part, 'tp', scatter_dimension=1, tiled=True)  19.3 us
    all_to_all x1, blocking collectives, body(): lax.all_to_all(packed.reshape(ep_count, capacity, sent_width), 'ep', spli...  12.8 us
    all_to_all x1, waiting for transfers between devices, body(): lax.all_to_all(expert_out.reshape(ep_count, capacity, own_width), 'ep', s...  6.86 us
    all_gather x1, blocking collectives, body(): expert_rows = lax.all_gather(expert_rows, 'tp', axis=1, tiled=True)  6.49 us
    psum x1, blocking collectives, body(): squares = lax.psum(jnp.sum(residual * residual, axis=-1), 'tp')  5.76 us
    dot_general x1, matrix products, body(): jnp.einsum('bkgl,bkdl->bkgd', past_prob.reshape(seq_count, kv_local, grou...  5.65 us
    all_to_all x1, starting transfers between devices, body(): lax.all_to_all(expert_out.reshape(ep_count, capacity, own_width), 'ep', s...  5.5 us
  transfers between devices with their start and end apart: 3, of which 3 were waited for; matrix products, arithmetic and copies ran while one was open for 1% of the time, Pallas kernels for 0%

commit v1 on v0

--- a/solution.py
+++ b/solution.py
@@ -88,7 +88,8 @@
         jnp.float32
     )
     residual = lax.dynamic_slice_in_dim(tokens_wide, column_start, own_width, 1) + attention
-    squares = lax.psum(jnp.sum(residual * residual, axis=-1), "tp")
+    row_data = jnp.sum(residual * residual, axis=-1)
+    squares = lax.all_gather(row_data, "tp").sum(axis=0)
     gain_part = lax.dynamic_slice_in_dim(post_gain, column_start, own_width, 0)
     expert_input = (residual * lax.rsqrt(squares / width + epsilon)[:, None] * gain_part).astype(
         jnp.bfloat16

time: 134 us -> 134 us (level)
    psum x1 -> x0, blocking collectives: 5.76 us -> none  [body(): squares = lax.psum(jnp.sum(residual * residual, axis=-1), 'tp')]
    unnamed x0 -> x1, blocking collectives: none -> 5.73 us
  transfers between devices with their start and end apart: 3 -> 3, of which waited for: 3 -> 3; matrix products, arithmetic and copies ran while one was open for 1% -> 2% of each run, Pallas kernels for 0% -> 0%
where the time goes in v1:
time: 134 us; the launch traced here: 133 us
  waiting for transfers between devices  46.1 us (34%)
  matrix products  27.8 us (21%)
  blocking collectives  25 us (19%)
  between operations  14.3 us (11%)
  other arithmetic  8.79 us (7%)
  local copies, waits for them, and re-layouts  5.73 us (4%)
  starting transfers between devices  5.55 us (4%)
    reduce_scatter x1, waiting for transfers between devices, body(): lax.psum_scatter(partial_value, 'tp', scatter_dimension=1, tiled=True)  19.9 us
    reduce_scatter x1, waiting for transfers between devices, body(): lax.psum_scatter(down_part, 'tp', scatter_dimension=1, tiled=True)  19.3 us
    all_to_all x1, blocking collectives, body(): lax.all_to_all(packed.reshape(ep_count, capacity, sent_width), 'ep', spli...  12.8 us
    all_to_all x1, waiting for transfers between devices, body(): lax.all_to_all(expert_out.reshape(ep_count, capacity, own_width), 'ep', s...  6.86 us
    all_gather x1, blocking collectives, body(): expert_rows = lax.all_gather(expert_rows, 'tp', axis=1, tiled=True)  6.49 us
    unnamed x1, blocking collectives  5.73 us
    dot_general x1, matrix products, body(): jnp.einsum('bkgl,bkdl->bkgd', past_prob.reshape(seq_count, kv_local, grou...  5.66 us
    all_to_all x1, starting transfers between devices, body(): lax.all_to_all(expert_out.reshape(ep_count, capacity, own_width), 'ep', s...  5.5 us
  transfers between devices with their start and end apart: 3, of which 3 were waited for; matrix products, arithmetic and copies ran while one was open for 2% of the time, Pallas kernels for 0%

profile of v1, /device:TPU:0, one launch (start us, length us, event | category | flops | bytes accessed | tf_op | source)
XLA Modules:
  0.0 133.3 jit_solution(3088765912253314386)
XLA Ops:
  6.5 0.8 broadcast_add_fusion
  7.3 0.7 iota_compare_fusion.1
  8.1 1.0 multiply_reduce_fusion
  9.1 0.1 iota_compare_fusion
  9.2 1.5 %select_reduce_fusion = f32[32,8]{1,0:T(8,128)S(1)} fusion(f32[32,8,1024]{2,1,0:T(8,128)} %param.27, pred[32,1024]{1,0:T(8,128)(4,1)S(1)} %iota_compare_fusion), kind=kLoop, calls=%fused_computation.25 | loop fusion | flops 524032 | bytes 1082368 | tf_op jit(solution)/shard_map/reduce_sum | solution.py:59
  10.8 1.1 fusion.43
  12.0 2.2 %convolution_convert_fusion.2 = bf16[32,512]{1,0:T(8,128)(2,1)S(1)} fusion(bf16[2048,512]{1,0:T(8,128)(2,1)} %param.20, f32[2048]{0:T(1024)} %param.18, f32[32]{0:T(128)S(1)} %add_rsqrt_fusion.1, bf16[32,2048]{1,0:T(8,128)(2,1)} %param.17), kind=kOutput, calls=%fused_computation.16 | convolution fusion | flops 67387392 | bytes 2269312 | tf_op jit(solution)/shard_map/dot_general | solution.py:47
  14.2 0.1 reshape.173
  14.3 4.6 %convolution_multiply_fusion = f32[32,2,4,1024]{3,2,1,0:T(4,128)S(1)} fusion(bf16[32,2,4,64]{3,2,1,0:T(4,128)(2,1)S(1)} %reshape.173, bf16[32,2,64,1024]{3,2,1,0:T(8,128)(2,1)} %param.25), kind=kOutput, calls=%fused_computation.8 | convolution fusion | flops 33816576 | bytes 9469952 | tf_op jit(solution)/shard_map/bkgd,bkdl->bkgl/dot_general | solution.py:54
  18.9 1.4 %mul.121 = f32[32,8,1024]{2,1,0:T(8,128)} reshape(f32[32,2,4,1024]{3,2,1,0:T(4,128)S(1)} %convolution_multiply_fusion) | data formatting | bytes 2097152 | tf_op jit(solution)/shard_map/mul | solution.py:60
  20.3 1.9 %fusion.54 = (f32[32,8]{1,0:T(8,128)S(1)}, f32[32,8,1024]{2,1,0:T(8,128)S(1)}) fusion(f32[32,8,1024]{2,1,0:T(8,128)} %param.27, f32[32,8,1024]{2,1,0:T(8,128)} %mul.121, f32[32,8]{1,0:T(8,128)S(1)} %copy.37, pred[32,1024]{1,0:T(8,128)(4,1)S(1)} %iota_compare_fusion.1), kind=kLoop, calls=%fused_computation.81 | loop fusion | flops 1048320 | bytes 3180544 | tf_op jit(solution)/shard_map/reduce_max | solution.py:68
  22.2 1.3 convolution_convert_fusion.5
  23.5 0.1 reshape.192
  23.6 0.2 fusion.55
  23.8 0.1 copy.48
  23.9 0.1 copy.39
  24.0 0.3 fusion.18
  24.5 1.1 divide_convert_fusion
  25.6 1.2 reshape.175
  26.8 0.1 copy.44
  26.9 1.3 fusion.17
  28.2 0.1 reshape.182
  28.4 5.7 %fusion.15 = bf16[32,2,4,64]{3,2,1,0:T(4,128)(2,1)S(1)} fusion(bf16[32,2,4,1024]{3,2,1,0:T(4,128)(2,1)S(1)} %reshape.175, bf16[32,2,64,1024]{3,2,1,0:T(8,128)(2,1)} %param.26, f32[32,2,64]{2,1,0:T(2,128)S(1)} %reshape.182, f32[32,2,4]{2,1,0:T(2,128)S(1)} %copy.44), kind=kOutput, calls=%fused_computation.13 | convolution fusion | flops 33603584 | bytes 8963072 | tf_op jit(solution)/shard_map/bkgl,bkdl->bkgd/dot_general | solution.py:74
  34.0 0.1 reshape.176
  34.2 1.1 convolution_convert_fusion
  35.3 0.1 copy.45
  35.4 0.1 reshape.177
  35.6 0.1 reduce_window_sum.11
  35.7 0.2 select_reduce_fusion.1
  35.9 0.6 dynamic-slice
  37.2 0.8 dynamic_slice.11
  38.0 19.9 %reduce-scatter.3.cloned.1.call-done = bf16[32,512]{1,0:T(8,128)(2,1)} async-done(((bf16[32,2048]{1,0:T(8,128)(2,1)}), bf16[32,512]{1,0:T(8,128)(2,1)}) %reduce-scatter.3.cloned.1.call-update) | async-done | bytes 32784 | tf_op jit(solution)/shard_map/reduce_scatter | solution.py:87
  57.9 0.9 multiply_reduce_fusion.1
  58.7 0.2 dynamic-update-slice
  59.0 5.7 %all-reduce = f32[128]{0:T(128)S(1)} all-reduce(f32[128]{0:T(128)S(1)} %dynamic-update-slice), channel_id=2, replica_groups=mesh['ep'=8,'tp'=4] {'tp'}, use_global_device_ids=true, to_apply=%add | all-reduce | flops 128 | bytes 1024
  64.7 0.1 reshape.183
  64.8 1.2 convolution_convert_fusion.1
  66.1 12.8 %all_to_all.10 = bf16[8,16,512]{2,1,0:T(8,128)(2,1)S(1)} all-to-all(bf16[8,16,512]{2,1,0:T(8,128)(2,1)S(1)} %bitcast.47), channel_id=1, replica_groups=mesh['ep'=8,'tp'=4] {'ep'}, dimensions={0} | all-to-all | bytes 262144 | tf_op jit(solution)/shard_map/all_to_all | solution.py:119
  78.9 6.5 %all_gather.11 = bf16[128,2048]{1,0:T(8,128)(2,1)S(1)} all-gather(bf16[128,512]{1,0:T(8,128)(2,1)S(1)} %bitcast.44), channel_id=1, replica_groups=mesh['ep'=8,'tp'=4] {'tp'}, dimensions={1}, use_global_device_ids=true | all-gather | bytes 655360 | tf_op jit(solution)/shard_map/all_gather | solution.py:127
  85.4 2.8 %fusion.4 = f32[128,896]{1,0:T(8,128)S(1)} fusion(bf16[128,2048]{1,0:T(8,128)(2,1)S(1)} %all_gather.11, bf16[1,2048,896]{2,1,0:T(8,128)(2,1)} %param.31), kind=kOutput, calls=%fused_computation.4 | convolution fusion | flops 469762048 | bytes 4653056 | tf_op jit(solution)/shard_map/dot_general | solution.py:128
  88.1 5.3 %fusion.6 = bf16[128,2048]{1,0:T(8,128)(2,1)} fusion(bf16[1,896,2048]{2,1,0:T(8,128)(2,1)} %param.33, bf16[128,2048]{1,0:T(8,128)(2,1)S(1)} %all_gather.11, bf16[1,2048,896]{2,1,0:T(8,128)(2,1)} %param.32, f32[128,896]{1,0:T(8,128)S(1)} %fusion.4), kind=kOutput, calls=%fused_computation.6 | convolution fusion | flops 940474368 | bytes 8847360 | tf_op jit(solution)/shard_map/dot_general | solution.py:131
  93.5 19.3 %reduce-scatter.5.cloned.1.call-done = bf16[128,512]{1,0:T(8,128)(2,1)} async-done(((bf16[128,2048]{1,0:T(8,128)(2,1)}), bf16[128,512]{1,0:T(8,128)(2,1)}) %reduce-scatter.5.cloned.1.call-update) | async-done | bytes 131088 | tf_op jit(solution)/shard_map/reduce_scatter | solution.py:135
  112.8 5.5 %all-to-all-start.1 = ((bf16[8,16,512]{2,1,0:T(8,128)(2,1)}), bf16[8,16,512]{2,1,0:T(8,128)(2,1)S(1)}, u32[]{:S(2)}, u32[]{:S(2)}) async-start(bf16[8,16,512]{2,1,0:T(8,128)(2,1)} %bitcast.46), calls=%async_computation.3 | async-start | bytes 262144 | tf_op jit(solution)/shard_map/all_to_all | solution.py:139
  118.3 0.1 copy.46
  118.4 0.1 mul.132
  118.5 0.3 fusion.29
  118.7 6.9 %all-to-all-done.1 = bf16[8,16,512]{2,1,0:T(8,128)(2,1)S(1)} async-done(((bf16[8,16,512]{2,1,0:T(8,128)(2,1)}), bf16[8,16,512]{2,1,0:T(8,128)(2,1)S(1)}, u32[]{:S(2)}, u32[]{:S(2)}) %all-to-all-start.1) | async-done | bytes 131104 | tf_op jit(solution)/shard_map/all_to_all | solution.py:139
  125.6 0.8 fusion.16
  (37 shorter events, 0.7 us)
Async XLA Ops:
  6.5 27.6 %copy-start = (bf16[512,2048]{1,0:T(8,128)(2,1)S(1)}, bf16[512,2048]{1,0:T(8,128)(2,1)}, u32[]{:S(2)}) copy-start(bf16[512,2048]{1,0:T(8,128)(2,1)} %param.24) | copy-start | bytes 6291460
  6.5 51.3 %reduce-scatter.3.cloned.1.call-start = ((), (), s32[]{:S(2)}) async-start(), calls=%async_computation.4 | async-start | bytes 163840 | tf_op jit(solution)/shard_map/reduce_scatter | solution.py:87
  18.9 3.3 %copy-start.1 = (bf16[32,2048]{1,0:T(8,128)(2,1)S(1)}, bf16[32,2048]{1,0:T(8,128)(2,1)}, u32[]{:S(2)}) copy-start(bf16[32,2048]{1,0:T(8,128)(2,1)} %param.17) | copy-start | bytes 393220
  18.9 3.3 %copy-start.3 = (f32[2048]{0:T(1024)S(1)}, f32[2048]{0:T(1024)}, u32[]{:S(2)}) copy-start(f32[2048]{0:T(1024)} %param.18) | copy-start | bytes 24580
  28.3 7.0 %copy-start.5 = (s32[32,2]{0,1:T(2,128)S(1)}, s32[32,2]{0,1:T(2,128)}, u32[]{:S(2)}) copy-start(s32[32,2]{0,1:T(2,128)} %param.29) | copy-start | bytes 772
  28.3 7.6 %copy-start.6 = (u32[32]{0:T(128)S(1)}, u32[32]{0:T(128)}, u32[]{:S(2)}) copy-start(u32[32]{0:T(128)} %constant.69) | copy-start | bytes 388
  35.3 77.5 %reduce-scatter.5.cloned.1.call-start = ((), (), s32[]{:S(2)}) async-start(), calls=%async_computation.5 | async-start | bytes 655360 | tf_op jit(solution)/shard_map/reduce_scatter | solution.py:135
  88.1 5.3 %copy-start.4 = (f32[32,2]{0,1:T(2,128)S(1)}, f32[32,2]{0,1:T(2,128)}, u32[]{:S(2)}) copy-start(f32[32,2]{0,1:T(2,128)} %param.30) | copy-start | bytes 772
  88.1 37.5 %copy-start.2 = (bf16[32,512]{1,0:T(8,128)(2,1)S(1)}, bf16[32,512]{1,0:T(8,128)(2,1)}, u32[]{:S(2)}) copy-start(bf16[32,512]{1,0:T(8,128)(2,1)} %reduce-scatter.3.cloned.1.call-done) | copy-start | bytes 98308
  112.8 12.8 %all-to-all-start.1 = ((bf16[8,16,512]{2,1,0:T(8,128)(2,1)}), bf16[8,16,512]{2,1,0:T(8,128)(2,1)S(1)}, u32[]{:S(2)}, u32[]{:S(2)}) async-start(bf16[8,16,512]{2,1,0:T(8,128)(2,1)} %bitcast.46), calls=%async_computation.3 | async-start | bytes 262144 | tf_op jit(solution)/shard_map/all_to_all | solution.py:139
Sparse Core Ops, SparseCore 0:
  35.4 22.4 reduce-scatter.2
  93.6 19.1 reduce-scatter.4
